TPU v7x, 32 devices: a whole 2x2x4 slice. The times are simulated.
32 devices in a mesh: sp: 16 (over z, y, x), tp: 2 (over core).
Axes of the slice: x: 2, y: 2, z: 4, core: 2. Of those that a mesh axis runs over, the one named last changes fastest.
Arguments:
- query_matrix: bfloat16 [4096, 2048], P('sp', 'tp'), may hold values from -6 to 6
- key_matrix: bfloat16 [4096, 2048], P('sp', 'tp'), may hold values from -6 to 6
- value_matrix: bfloat16 [4096, 2048], P('sp', 'tp'), may hold values from -6 to 6
- output_gate_logits: bfloat16 [4096, 2048], P('sp', 'tp'), may hold values from -6 to 6
- decay_preactivation: bfloat16 [4096, 2048], P('sp', 'tp'), may hold values from -3 to 12
- head_extra_decay: float32 [4096, 32], P('sp', 'tp'), may hold values from -0.7 to 0
- residual: bfloat16 [4096, 2048], P(('sp', 'tp')), may hold values from -6 to 6
- head_norm_gain: float32 [64], replicated, may hold values from 0.1 to 1.9
- output_projection_weight: bfloat16 [2048, 2048], P('tp'), may hold values from -0.125 to 0.125
- mixer_norm_gain: float32 [2048], replicated, may hold values from 0.1 to 1.9
- routes: int32 [4096, 2], P(('sp', 'tp')), may hold values from 0 to 15, all different within a row; in each aligned block of 128 rows (0 to 127, 128 to 255, ...) at most 32 rows name the same one
- routing_weight: float32 [4096, 2], P(('sp', 'tp')), may hold values from 0.2 to 1.5
- routed_gate_weight: bfloat16 [16, 2048, 1024], P('sp', None, 'tp'), may hold values from -0.125 to 0.125
- routed_up_weight: bfloat16 [16, 2048, 1024], P('sp', None, 'tp'), may hold values from -0.125 to 0.125
- routed_down_weight: bfloat16 [16, 1024, 2048], P('sp', 'tp'), may hold values from -0.1875 to 0.1875
- common_gate_weight: bfloat16 [2048, 512], replicated, may hold values from -0.125 to 0.125
- common_up_weight: bfloat16 [2048, 512], replicated, may hold values from -0.125 to 0.125
- common_down_weight: bfloat16 [512, 2048], replicated, may hold values from -0.25 to 0.25
- final_norm_gain: float32 [2048], replicated, may hold values from 0.1 to 1.9
Outputs:
- layer_out: bfloat16 [4096, 2048], P(('sp', 'tp'))
Inputs may be any that keep to these rules, and one draw needn't show every extreme that they name: `routes`: each row names 2 different experts. In the rows of one device (aligned blocks of rows) no expert is named by more than 32 rows, a bound that some block reaches.
All inputs are finite; a program needn't handle non-finite values.
Results may differ from a plain program's by a relative error of at most 0.019.
Values may be sent and summed in bfloat16 or wider, within the bound.
A program may use at most 192 MiB of HBM per device.

v0:
```python
import jax
import jax.numpy as jnp
from jax import lax
from jax.sharding import PartitionSpec as P

HEAD_NUMBER = 32
KEY_HEAD_SIZE = 64
BLOCK_TOKENS = 64


EPS = 1e-06
GATE_DIVISOR = 16.0


def entering(shard, axis, combine, identity, reverse):
    devices, place = (lax.axis_size(axis), lax.axis_index(axis))
    everything = jax.tree.map(
        lambda part, kind: lax.all_gather(part.astype(kind), axis),
        shard,
        (jnp.bfloat16, jnp.bfloat16),
    )
    start = jax.tree.map(
        lambda part, zero: jnp.broadcast_to(jnp.asarray(zero, part.dtype), part.shape),
        shard,
        identity,
    )

    def step(k, before):
        at = devices - 1 - k if reverse else k
        reached = at > place if reverse else at < place
        new = combine(
            before, jax.tree.map(lambda part, own: part[at].astype(own.dtype), everything, shard)
        )
        return jax.tree.map(lambda a, b: jnp.where(reached, a, b), new, before)

    return lax.fori_loop(0, devices, step, start)


def layer_norm(values, gain):
    center = values - jnp.mean(values, axis=-1, keepdims=True)
    spread = jnp.mean(center * center, axis=-1, keepdims=True)
    return center * lax.rsqrt(spread + EPS) * gain


def carry_combine(earlier, later):
    return (earlier[0] + later[0], jnp.exp(later[0])[..., None] * earlier[1] + later[1])


def block_products(
    query_matrix, key_matrix, value_matrix, decay_preactivation, head_extra_decay, number_of_heads
):
    token_count = query_matrix.shape[0]
    number_of_blocks = token_count // BLOCK_TOKENS
    blocked_layout = (number_of_blocks, BLOCK_TOKENS, number_of_heads, KEY_HEAD_SIZE)
    logarithm_decay = jax.nn.log_sigmoid(decay_preactivation.astype(jnp.float32)).reshape(
        token_count, number_of_heads, KEY_HEAD_SIZE
    )
    logarithm_decay = (logarithm_decay / GATE_DIVISOR + head_extra_decay[:, :, None]).reshape(
        blocked_layout
    )
    inside_block = jnp.cumsum(logarithm_decay, axis=1)
    block_total = inside_block[:, -1]
    query_float = query_matrix.astype(jnp.float32).reshape(blocked_layout) * KEY_HEAD_SIZE ** (-0.5)
    key_float = key_matrix.astype(jnp.float32).reshape(blocked_layout)
    value_f = value_matrix.astype(jnp.float32).reshape(blocked_layout)
    query_up = query_float * jnp.exp(inside_block)
    query_down = query_float * jnp.exp(-inside_block)
    key_up = key_float * jnp.exp(inside_block)
    key_down = key_float * jnp.exp(-inside_block)
    lower_mask = jnp.tril(jnp.ones((BLOCK_TOKENS, BLOCK_TOKENS), bool))
    ahead = jnp.einsum("nihc,njhc->nhij", query_up, key_down)
    behind = jnp.einsum("nihc,njhc->nhij", query_down, key_up)
    scores = jnp.where(lower_mask, ahead, 0.0) + jnp.where(lower_mask, 0.0, behind)
    local_out = jnp.einsum("nhij,njhv->nihv", scores, value_f)
    key_end = key_float * jnp.exp(block_total[:, None] - inside_block)
    left_sum = jnp.einsum("njhc,njhv->nhcv", key_end, value_f)
    right_sum = jnp.einsum("njhc,njhv->nhcv", key_up, value_f)

    def carry_step(carried, fragments):
        total, summed = fragments
        return (jnp.exp(total)[..., None] * carried + summed, carried)

    zero_state = jnp.zeros(left_sum.shape[1:], jnp.float32)
    left_dev, left_before = lax.scan(carry_step, zero_state, (block_total, left_sum))
    right_dev, right_after = lax.scan(
        carry_step, zero_state, (block_total, right_sum), reverse=True
    )
    query_tail = query_float * jnp.exp(block_total[:, None] - inside_block)
    local_out = local_out + jnp.einsum("nihc,nhcv->nihv", query_up, left_before)
    local_out = local_out + jnp.einsum("nihc,nhcv->nihv", query_tail, right_after)
    before_blocks = jnp.cumsum(block_total, axis=0) - block_total
    device_total = jnp.sum(block_total, axis=0)
    from_start = inside_block + before_blocks[:, None]
    query_head = query_float * jnp.exp(from_start)
    query_rest = query_float * jnp.exp(device_total[None, None] - from_start)
    return (local_out, query_head, query_rest, device_total, left_dev, right_dev)


def expert_half(arrived, gate_half, up_half, down_half):
    flat_rows = arrived.reshape(-1, arrived.shape[-1])
    gate_part = jnp.dot(flat_rows, gate_half, preferred_element_type=jnp.float32)
    up_part = jnp.dot(flat_rows, up_half, preferred_element_type=jnp.float32)
    inner = (jax.nn.silu(gate_part) * up_part).astype(jnp.bfloat16)
    partial_out = jnp.dot(inner, down_half, preferred_element_type=jnp.float32).astype(jnp.bfloat16)
    return partial_out.reshape(arrived.shape)


def per_device(
    query_matrix,
    key_matrix,
    value_matrix,
    output_gate_logits,
    decay_preactivation,
    head_extra_decay,
    residual,
    head_norm_gain,
    output_projection_weight,
    mixer_norm_gain,
    routes,
    routing_weight,
    routed_gate_weight,
    routed_up_weight,
    routed_down_weight,
    common_gate_weight,
    common_up_weight,
    common_down_weight,
    final_norm_gain,
):
    tp_size = lax.axis_size("tp")
    number_of_heads = HEAD_NUMBER // tp_size
    token_count = query_matrix.shape[0]
    local_out, query_head, query_rest, device_total, left_dev, right_dev = block_products(
        query_matrix,
        key_matrix,
        value_matrix,
        decay_preactivation,
        head_extra_decay,
        number_of_heads,
    )
    identity = (jnp.zeros_like(device_total), jnp.zeros_like(left_dev))
    left_in = entering((device_total, left_dev), "sp", carry_combine, identity, False)[1]
    right_in = entering((device_total, right_dev), "sp", carry_combine, identity, True)[1]
    mixed = local_out + jnp.einsum("nihc,hcv->nihv", query_head, left_in)
    mixed = mixed + jnp.einsum("nihc,hcv->nihv", query_rest, right_in)
    mixed = mixed.reshape(token_count, number_of_heads, KEY_HEAD_SIZE)
    normed_heads = (
        mixed * lax.rsqrt(jnp.mean(mixed * mixed, axis=-1, keepdims=True) + EPS) * head_norm_gain
    )
    gated = (
        normed_heads.reshape(token_count, number_of_heads * KEY_HEAD_SIZE)
        * jax.nn.silu(output_gate_logits.astype(jnp.float32))
    ).astype(jnp.bfloat16)
    projected = lax.psum_scatter(
        jnp.dot(gated, output_projection_weight, preferred_element_type=jnp.float32).astype(
            jnp.bfloat16
        ),
        "tp",
        scatter_dimension=0,
        tiled=True,
    ).astype(jnp.float32)
    normed = layer_norm(residual.astype(jnp.float32) + projected, mixer_norm_gain).astype(
        jnp.bfloat16
    )
    row_count = normed.shape[0]
    model_width = normed.shape[1]
    top_count = routes.shape[1]
    experts = lax.axis_size("sp")
    capacity = max(2, row_count * top_count // experts * 2)
    flat_expert = routes.reshape(-1)
    member = (flat_expert[:, None] == jnp.arange(experts, dtype=jnp.int32)[None, :]).astype(
        jnp.int32
    )
    rank_in = jnp.sum((jnp.cumsum(member, axis=0) - member) * member, axis=1)
    slot_of = flat_expert * capacity + rank_in
    source_row = (
        jnp.zeros((experts * capacity,), jnp.int32)
        .at[slot_of]
        .set(jnp.arange(row_count * top_count, dtype=jnp.int32) // top_count)
    )
    outbound = normed[source_row].reshape(experts, capacity, model_width)
    gate_half = routed_gate_weight[0]
    up_half = routed_up_weight[0]
    down_half = routed_down_weight[0]
    paired = lax.all_gather(
        lax.all_to_all(outbound, "sp", split_axis=0, concat_axis=0, tiled=True),
        "tp",
        axis=0,
        tiled=True,
    )
    partial_out = expert_half(paired, gate_half, up_half, down_half).astype(jnp.float32)
    summed = lax.psum_scatter(
        partial_out.astype(jnp.bfloat16), "tp", scatter_dimension=0, tiled=True
    )
    expert_out = lax.all_to_all(summed, "sp", split_axis=0, concat_axis=0, tiled=True)
    flat_out = expert_out.reshape(experts * capacity, model_width)
    picked = flat_out[slot_of].astype(jnp.float32).reshape(row_count, top_count, model_width)
    routed = jnp.einsum("rk,rkd->rd", routing_weight, picked)
    shared_gate_out = jnp.dot(normed, common_gate_weight, preferred_element_type=jnp.float32)
    shared_up_out = jnp.dot(normed, common_up_weight, preferred_element_type=jnp.float32)
    shared_inner = (jax.nn.silu(shared_gate_out) * shared_up_out).astype(jnp.bfloat16)
    feed = jnp.dot(shared_inner, common_down_weight, preferred_element_type=jnp.float32) + routed
    return layer_norm(normed.astype(jnp.float32) + feed, final_norm_gain).astype(jnp.bfloat16)


def solution(mesh):
    placed = (
        P("sp", "tp"),
        P("sp", "tp"),
        P("sp", "tp"),
        P("sp", "tp"),
        P("sp", "tp"),
        P("sp", "tp"),
        P(("sp", "tp"), None),
        P(),
        P("tp", None),
        P(),
        P(("sp", "tp"), None),
        P(("sp", "tp"), None),
        P("sp", None, "tp"),
        P("sp", None, "tp"),
        P("sp", "tp", None),
        P(),
        P(),
        P(),
        P(),
    )
    return jax.shard_map(
        per_device, mesh=mesh, in_specs=placed, out_specs=P(("sp", "tp"), None), check_vma=False
    )
```

profile of v0, /device:TPU:0, one launch (start us, length us, event | category | flops | bytes accessed | tf_op | source)
XLA Modules:
  0.0 428.9 jit_solution(7121600153168388314)
XLA Ops:
  19.6 5.8 %exponential_multiply_fusion.1 = (bf16[4,64,16,64]{3,2,1,0:T(8,128)(2,1)}, bf16[4,64,16,64]{3,2,1,0:T(8,128)(2,1)}, bf16[4,64,16,64]{3,2,1,0:T(8,128)(2,1)}, bf1...) fusion(f32[4,64,16,64]{3,2,1,0:T(8,128)} %mul.221, ...), kind=kLoop, calls=%fused_computation.44 | loop fusion | flops 5242880 | bytes 7376896 | tf_op jit(solution)/shard_map/mul | solution.py:94
  34.5 8.5 %while.61 = (s32[]{:T(128)}, f32[16,64,64]{2,1,0:T(8,128)S(1)}, bf16[4,16,64,64]{3,2,1,0:T(8,128)(2,1)}, f32[4,16,64]{2,1,0:T(8,128)S(1)}, f32[4,16,64,64]{3,2,1,0:T(8,128)}, /*index=5*/s32[]{:T(128)}, s32[]{:T(128)}, s32[]{:T(128)}) while((s32[]{:T(128)}, f32[16,64,64]{2,1,0:T(8,128)S(1)}, bf16[4,16,64,64]{3,2,1,0:T(8,128)(2,1)}, ...), condition=%wide.region_4.5_spmd.clone, body=%wide.region_3.4_spmd.clone.sunk | while | flops 262148 | bytes 1323128 | solution.py:85
  43.8 3.4 fusion.14
  48.5 8.5 %while.60 = (s32[]{:T(128)}, f32[16,64,64]{2,1,0:T(8,128)S(1)}, bf16[4,16,64,64]{3,2,1,0:T(8,128)(2,1)}, f32[4,16,64]{2,1,0:T(8,128)S(1)}, f32[4,16,64,64]{3,2,1,0:T(8,128)}, /*index=5*/s32[]{:T(128)}, s32[]{:T(128)}) while((s32[]{:T(128)}, f32[16,64,64]{2,1,0:T(8,128)S(1)}, bf16[4,16,64,64]{3,2,1,0:T(8,128)(2,1)}, ...), condition=%wide.region_2.3_spmd.clone, body=%wide.region_1.2_spmd.clone.sunk | while | flops 262147 | bytes 1323616 | solution.py:84
  61.3 43.6 %all-gather = bf16[256,64]{1,0:T(8,128)(2,1)S(1)} all-gather(bf16[16,64]{1,0:T(8,128)(2,1)S(1)} %convert_element_type.124), channel_id=2, replica_groups=mesh['sp'=16,'tp'=2] {'sp'}, dimensions={0}, use_global_device_ids=true | all-gather | bytes 34816 | tf_op jit(solution)/shard_map/all_gather | solution.py:18
  105.0 3.7 fusion.12
  108.7 5.1 %fusion.20 = f32[4,16,64,64]{2,3,1,0:T(8,128)} fusion(f32[4,16,64,64]{3,2,1,0:T(8,128)} %fusion.16, bf16[4,64,16,64]{3,2,1,0:T(8,128)(2,1)} %get-tuple-element.491, bf16[4,64,16,64]{3,2,1,0:T(8,128)(2,1)} %get-tuple-element.483, pred[64,64]{1,0:T(8,128)(4,1)S(1)} %iota_compare_fusion, bf16[4,64,16,64]{3,2,1,0:T(8,128)(2,1)} %reshape.191), kind=kOutput, calls=%fused_computation.46 | convolution fusion | flops 68157440 | bytes 3674112 | tf_op jit(solution)/shard_map/nhij,njhv->nihv/dot_general | solution.py:74
  113.8 8.8 %all-gather.11.cloned.1.call-done = bf16[256,64,64]{2,1,0:T(8,128)(2,1)} async-done(((bf16[16,64,64]{2,1,0:T(8,128)(2,1)}), bf16[256,64,64]{2,1,0:T(8,128)(2,1)}) %all-gather.11.cloned.1.call-update) | async-done | bytes 2097168 | tf_op jit(solution)/shard_map/all_gather | solution.py:18
  122.5 21.7 %while.63 = (s32[]{:T(128)}, f32[16,64,64]{2,1,0:T(8,128)S(1)}, s32[]{:T(128)}, bf16[16,16,64]{2,1,0:T(8,128)(2,1)S(1)}, bf16[16,16,64,64]{3,2,1,0:T(8,128)(2,1)...) while((s32[]{:T(128)}, f32[16,64,64]{2,1,0:T(8,128)S(1)}, s32[]{:T(128)}, ...), condition=%wide.region_10.11_spmd.clone, body=%wide.region_9.10_spmd.clone.sunk | while | flops 328712 | bytes 665767 | solution.py:36
  144.2 55.4 %all-gather.9.cloned.1.call-done = bf16[256,64,64]{2,1,0:T(8,128)(2,1)} async-done(((bf16[16,64,64]{2,1,0:T(8,128)(2,1)}), bf16[256,64,64]{2,1,0:T(8,128)(2,1)}) %all-gather.9.cloned.1.call-update) | async-done | bytes 2097168 | tf_op jit(solution)/shard_map/all_gather | solution.py:18
  199.6 21.4 %while.62 = (s32[]{:T(128)}, f32[16,64,64]{2,1,0:T(8,128)S(1)}, s32[]{:T(128)}, bf16[16,16,64]{2,1,0:T(8,128)(2,1)S(1)}, bf16[16,16,64,64]{3,2,1,0:T(8,128)(2,1)}, /*index=5*/s32[]{:T(128)}, s32[]{:T(128)}) while((s32[]{:T(128)}, f32[16,64,64]{2,1,0:T(8,128)S(1)}, s32[]{:T(128)}, bf16[16,16,64]{2,1,0:T(8,128)(2,1)S(1)}, ...), condition=%wide.region_7.8_spmd.clone, body=%wide.region_6.7_spmd.clone.sunk | while | flops 328708 | bytes 665705 | solution.py:36
  235.2 5.4 %convolution_convert_fusion.1 = bf16[256,2048]{1,0:T(8,128)(2,1)} fusion(bf16[1024,2048]{1,0:T(8,128)(2,1)} %param.35, bf16[256,1024]{1,0:T(8,128)(2,1)} %param.30, f32[256,1024]{1,0:T(8,128)} %reshape.192, f32[256,1024]{1,0:T(8,128)} %copy.102, f32[1024]{0:T(1024)S(1)} %mul.235), kind=kOutput, calls=%fused_computation.17 | convolution fusion | flops 1076625408 | bytes 7868416 | tf_op jit(solution)/shard_map/dot_general | solution.py:154
  243.8 4.1 reduce-scatter.3.cloned.1.call-done
  250.8 3.3 gather_fusion
  254.2 56.1 %all_to_all.10 = bf16[16,32,2048]{2,1,0:T(8,128)(2,1)} all-to-all(bf16[16,32,2048]{2,1,0:T(8,128)(2,1)} %bitcast.150), channel_id=1, replica_groups=mesh['sp'=16,'tp'=2] {'sp'}, dimensions={0} | all-to-all | bytes 4194304 | tf_op jit(solution)/shard_map/all_to_all | solution.py:185
  310.6 11.9 %all-gather.7.cloned.1.call-done = bf16[32,32,2048]{2,1,0:T(8,128)(2,1)} async-done(((bf16[16,32,2048]{2,1,0:T(8,128)(2,1)}), bf16[32,32,2048]{2,1,0:T(8,128)(2,1)}) %all-gather.7.cloned.1.call-update) | async-done | bytes 4194320 | tf_op jit(solution)/shard_map/all_gather | solution.py:184
  322.5 6.6 %fusion.4 = f32[1024,512]{1,0:T(8,128)} fusion(bf16[1024,2048]{1,0:T(8,128)(2,1)} %bitcast.161, bf16[1,2048,512]{2,1,0:T(8,128)(2,1)} %param.40), kind=kOutput, calls=%fused_computation.21 | convolution fusion | flops 2147483648 | bytes 8388608 | tf_op jit(solution)/shard_map/dot_general | solution.py:102
  329.1 10.1 %convolution_convert_fusion = bf16[1024,2048]{1,0:T(8,128)(2,1)} fusion(bf16[1,512,2048]{2,1,0:T(8,128)(2,1)S(1)} %copy-done, f32[1024,512]{1,0:T(8,128)} %fusion.4, bf16[1024,2048]{1,0:T(8,128)(2,1)} %bitcast.162, bf16[1,2048,512]{2,1,0:T(8,128)(2,1)} %param.39), kind=kOutput, calls=%fused_computation.15 | convolution fusion | flops 4300210176 | bytes 14680064 | tf_op jit(solution)/shard_map/dot_general | solution.py:104
  339.2 13.4 %reduce-scatter.5.cloned.1.call-done = bf16[16,32,2048]{2,1,0:T(8,128)(2,1)} async-done(((bf16[32,32,2048]{2,1,0:T(8,128)(2,1)}), bf16[16,32,2048]{2,1,0:T(8,128)(2,1)}) %reduce-scatter.5.cloned.1.call-update) | async-done | bytes 2097168 | tf_op jit(solution)/shard_map/reduce_scatter | solution.py:191
  352.6 7.0 %all-to-all-start.1 = ((bf16[16,32,2048]{2,1,0:T(8,128)(2,1)}), bf16[16,32,2048]{2,1,0:T(8,128)(2,1)}, u32[]{:S(2)}, u32[]{:S(2)}) async-start(bf16[16,32,2048]{2,1,0:T(8,128)(2,1)} %reduce-scatter.5.cloned.1.call-done), calls=%async_computation.3 | async-start | bytes 4194304 | tf_op jit(solution)/shard_map/all_to_all | solution.py:194
  361.7 41.1 %all-to-all-done.1 = bf16[16,32,2048]{2,1,0:T(8,128)(2,1)} async-done(((bf16[16,32,2048]{2,1,0:T(8,128)(2,1)}), bf16[16,32,2048]{2,1,0:T(8,128)(2,1)}, u32[]{:S(2)}, u32[]{:S(2)}) %all-to-all-start.1) | async-done | bytes 2097184 | tf_op jit(solution)/shard_map/all_to_all | solution.py:194
  402.8 5.2 %gather_fusion.1 = bf16[256,2048]{1,0:T(8,128)(2,1)} fusion(bf16[512,2048]{1,0:T(8,128)(2,1)} %bitcast.23, s32[1024]{0:T(1024)S(1)} %pad_clamp_fusion), kind=kCustom, calls=%fused_computation.1 | custom fusion | bytes 2098176 | tf_op jit(solution)/shard_map/gather | solution.py:196
  410.6 3.5 fusion.95
  414.1 4.6 %fusion.89 = (f32[128]{0:T(128)S(1)}, f32[128,2048]{1,0:T(8,128)}) fusion(f32[128,1,2048]{2,1,0:T(1,128)} %fusion.95, bf16[512,2048]{1,0:T(8,128)(2,1)} %param.44, bf16[128,2048]{1,0:T(8,128)(2,1)S(1)} %multiply_convert_fusion.2, bf16[2048,512]{1,0:T(8,128)(2,1)} %param.43, f32[128,512]{1,0:T(8,128)S(1)} %fusion.94), kind=kOutput, calls=%fused_computation.133 | convolution fusion | flops 538312576 | bytes 7078400 | tf_op jit(solution)/shard_map/dot_general | solution.py:201
  (199 shorter events, 116.0 us)
Async XLA Ops:
  6.5 322.5 %copy-start = (bf16[1,512,2048]{2,1,0:T(8,128)(2,1)S(1)}, bf16[1,512,2048]{2,1,0:T(8,128)(2,1)}, u32[]{:S(2)}) copy-start(bf16[1,512,2048]{2,1,0:T(8,128)(2,1)} %param.41) | copy-start | bytes 6291460
  6.5 3.8 copy-start.12
  6.5 116.0 %all-gather.11.cloned.1.call-start = ((), (), s32[]{:S(2)}) async-start(), calls=%async_computation.8 | async-start | bytes 4456448 | tf_op jit(solution)/shard_map/all_gather | solution.py:18
  10.4 3.4 copy-start.9
  12.4 1.4 copy-start.2
  14.9 2.9 copy-start.10
  25.4 2.8 copy-start.11
  43.8 155.8 %all-gather.9.cloned.1.call-start = ((), (), s32[]{:S(2)}) async-start(), calls=%async_computation.7 | async-start | bytes 4456448 | tf_op jit(solution)/shard_map/all_gather | solution.py:18
  57.8 190.0 %reduce-scatter.3.cloned.1.call-start = ((), (), s32[]{:S(2)}) async-start(), calls=%async_computation.4 | async-start | bytes 1572864 | tf_op jit(solution)/shard_map/reduce_scatter | solution.py:153
  57.9 47.0 %copy-start.17 = (f32[64]{0:T(128)S(1)}, f32[64]{0:T(128)}, u32[]{:S(2)}) copy-start(f32[64]{0:T(128)} %param.34) | copy-start | bytes 772
  221.0 2.6 copy-start.7
  221.0 3.7 copy-start.4
  221.0 3.7 copy-start.8
  223.6 1.2 copy-start.1
  223.6 1.9 copy-start.3
  235.2 5.5 %copy-start.15 = (s32[128,2]{0,1:T(2,128)S(1)}, s32[128,2]{0,1:T(2,128)}, u32[]{:S(2)}) copy-start(s32[128,2]{0,1:T(2,128)} %param.37) | copy-start | bytes 3076
  235.2 12.6 %copy-start.5 = (bf16[128,2048]{1,0:T(8,128)(2,1)S(1)}, bf16[128,2048]{1,0:T(8,128)(2,1)}, u32[]{:S(2)}) copy-start(bf16[128,2048]{1,0:T(8,128)(2,1)} %param.33) | copy-start | bytes 1572868
  240.6 9.9 %copy-start.13 = (f32[2048]{0:T(1024)S(1)}, f32[2048]{0:T(1024)}, u32[]{:S(2)}) copy-start(f32[2048]{0:T(1024)} %param.36) | copy-start | bytes 24580
  240.7 81.8 %all-gather.7.cloned.1.call-start = ((), (), s32[]{:S(2)}) async-start(), calls=%async_computation.5 | async-start | bytes 6291456 | tf_op jit(solution)/shard_map/all_gather | solution.py:184
  247.8 2.7 copy-start.6
  310.3 42.2 %reduce-scatter.5.cloned.1.call-start = ((), (), s32[]{:S(2)}) async-start(), calls=%async_computation.6 | async-start | bytes 6291456 | tf_op jit(solution)/shard_map/reduce_scatter | solution.py:191
  339.2 20.3 %copy-start.16 = (f32[128,2]{0,1:T(2,128)S(1)}, f32[128,2]{0,1:T(2,128)}, u32[]{:S(2)}) copy-start(f32[128,2]{0,1:T(2,128)} %param.38) | copy-start | bytes 3076
  352.6 50.3 %all-to-all-start.1 = ((bf16[16,32,2048]{2,1,0:T(8,128)(2,1)}), bf16[16,32,2048]{2,1,0:T(8,128)(2,1)}, u32[]{:S(2)}, u32[]{:S(2)}) async-start(bf16[16,32,2048]{2,1,0:T(8,128)(2,1)} %reduce-scatter.5.cloned.1.call-done), calls=%async_computation.3 | async-start | bytes 4194304 | tf_op jit(solution)/shard_map/all_to_all | solution.py:194
  414.1 6.1 %copy-start.14 = (f32[2048]{0:T(1024)S(1)}, f32[2048]{0:T(1024)}, u32[]{:S(2)}) copy-start(f32[2048]{0:T(1024)} %param.45) | copy-start | bytes 24580
Sparse Core Ops, SparseCore 0:
  43.9 78.6 all-gather.10
  125.3 74.2 all-gather.8
  240.8 6.9 reduce-scatter.2
  310.4 11.9 all-gather.6
  339.3 13.2 reduce-scatter.4
where the time goes:
time: 435 us; the launch traced here: 429 us
  waiting for transfers between devices  135 us (31%)
  blocking collectives  99.8 us (23%)
  other arithmetic  78.4 us (18%)
  matrix products  57 us (13%)
  local copies, waits for them, and re-layouts  36.9 us (8%)
  between operations  13.5 us (3%)
  starting transfers between devices  7.35 us (2%)
    all_gather x2, waiting for transfers between devices, entering(): lax.all_gather(part.astype(kind), axis)  64.1 us
    all_to_all x1, blocking collectives, per_device(): lax.all_to_all(outbound, 'sp', split_axis=0, concat_axis=0, tiled=True)  56.1 us
    all_gather x1, blocking collectives, entering(): lax.all_gather(part.astype(kind), axis)  43.6 us
    select_n x32, other arithmetic, step(): return jax.tree.map(lambda a, b: jnp.where(reached, a, b), new, before)  41.5 us
    all_to_all x1, waiting for transfers between devices, per_device(): lax.all_to_all(summed, 'sp', split_axis=0, concat_axis=0, tiled=True)  41.1 us
    reduce_scatter x1, waiting for transfers between devices, per_device(): lax.psum_scatter(partial_out.astype(jnp.bfloat16), 'tp', scatter_dimensio...  13.4 us
    all_gather x1, waiting for transfers between devices, per_device(): lax.all_gather(lax.all_to_all(outbound, 'sp', split_axis=0, concat_axis=0...  11.9 us
    add x8, other arithmetic, carry_step(): return (jnp.exp(total)[..., None] * carried + summed, carried)  10.7 us
  transfers between devices with their start and end apart: 6, of which 6 were waited for; matrix products, arithmetic and copies ran while one was open for 12% of the time, Pallas kernels for 0%

commit v1 on v0

v1 whole, which is shorter than its diff:
```python
import functools

import jax
import jax.numpy as jnp
from jax import lax
from jax.experimental import pallas as pl
from jax.experimental.pallas import tpu as pltpu
from jax.sharding import PartitionSpec as P

KEY_HEAD_SIZE = 64
BLOCK_TOKENS = 64


EPS = 1e-06
GATE_DIVISOR = 16.0


def layer_norm(values, gain):
    center = values - jnp.mean(values, axis=-1, keepdims=True)
    spread = jnp.mean(center * center, axis=-1, keepdims=True)
    return center * lax.rsqrt(spread + EPS) * gain


LANES = 128
MESH = pl.DeviceIdType.MESH


def lane_half(rows):
    return lax.broadcasted_iota(jnp.int32, (rows, LANES), 1) < KEY_HEAD_SIZE


def local_kernel(q_ref, k_ref, v_ref, decay_ref, extra_ref, out_ref, wide_ref, state_ref, total_ref):
    pair = pl.program_id(0)
    tokens = q_ref.shape[0]
    heads = extra_ref.shape[1]
    block = BLOCK_TOKENS
    half = lane_half(tokens)
    decay = decay_ref[...].astype(jnp.float32)
    logarithm = jnp.minimum(decay, 0.0) - jnp.log1p(jnp.exp(-jnp.abs(decay)))
    row = lax.broadcasted_iota(jnp.int32, (heads, LANES), 0)
    lane = lax.broadcasted_iota(jnp.int32, (heads, LANES), 1)
    chosen = (row == pair * (LANES // KEY_HEAD_SIZE) + lane // KEY_HEAD_SIZE).astype(jnp.float32)
    extra = jnp.dot(
        extra_ref[...], chosen, precision=lax.Precision.HIGHEST, preferred_element_type=jnp.float32
    )
    logarithm = logarithm * (1.0 / GATE_DIVISOR) + extra
    at = lax.broadcasted_iota(jnp.int32, (tokens, tokens), 0)
    other = lax.broadcasted_iota(jnp.int32, (tokens, tokens), 1)
    summed = jnp.dot(
        (other <= at).astype(jnp.float32),
        logarithm,
        precision=lax.Precision.HIGHEST,
        preferred_element_type=jnp.float32,
    )
    total = summed[tokens - 1 : tokens]
    query = q_ref[...].astype(jnp.float32) * KEY_HEAD_SIZE ** (-0.5)
    key = k_ref[...].astype(jnp.float32)
    value = v_ref[...]
    grown, rest = jnp.exp(summed), jnp.exp(total - summed)
    wide_ref[:, :LANES] = (query * grown).astype(jnp.bfloat16)
    wide_ref[:, LANES:] = (query * rest).astype(jnp.bfloat16)
    over = (((0,), (0,)), ((), ()))
    left = lax.dot_general(
        (key * rest).astype(jnp.bfloat16), value, over, preferred_element_type=jnp.float32
    )
    right = lax.dot_general(
        (key * grown).astype(jnp.bfloat16), value, over, preferred_element_type=jnp.float32
    )
    few = lane_half(KEY_HEAD_SIZE)
    top, low = slice(0, KEY_HEAD_SIZE), slice(KEY_HEAD_SIZE, LANES)
    first = jnp.where(few, left[top], pltpu.roll(right[top], KEY_HEAD_SIZE, 1))
    second = jnp.where(few, pltpu.roll(left[low], KEY_HEAD_SIZE, 1), right[low])
    state_ref[top] = first.astype(jnp.bfloat16)
    state_ref[low] = second.astype(jnp.bfloat16)
    total_ref[0] = total
    apart = (((1,), (1,)), ((), ()))
    small = lane_half(block)
    for place in range(tokens // block):
        begin, end = place * block, (place + 1) * block
        own = summed[begin:end]
        before = summed[begin - 1 : begin] if place else jnp.zeros((1, LANES), jnp.float32)
        after = summed[end - 1 : end]
        mine = query[begin:end]
        ups = mine * jnp.exp(own - before)
        tails = mine * jnp.exp(after - own)
        ups = jnp.concatenate([jnp.where(small, ups, 0.0), jnp.where(small, 0.0, ups)], axis=0)
        tails = jnp.concatenate(
            [jnp.where(small, tails, 0.0), jnp.where(small, 0.0, tails)], axis=0
        )
        key_left = key * jnp.exp(jnp.minimum(before - summed, 64.0))
        key_right = key * jnp.exp(jnp.minimum(summed - after, 64.0))
        ahead = lax.dot_general(
            ups.astype(jnp.bfloat16),
            key_left.astype(jnp.bfloat16),
            apart,
            preferred_element_type=jnp.float32,
        )
        behind = lax.dot_general(
            tails.astype(jnp.bfloat16),
            key_right.astype(jnp.bfloat16),
            apart,
            preferred_element_type=jnp.float32,
        )
        here = lax.broadcasted_iota(jnp.int32, (2 * block, tokens), 0)
        here = jnp.where(here < block, here, here - block) + begin
        there = lax.broadcasted_iota(jnp.int32, (2 * block, tokens), 1)
        scores = jnp.where(there <= here, ahead, behind).astype(jnp.bfloat16)
        both = jnp.dot(scores, value, preferred_element_type=jnp.float32)
        out_ref[begin:end] = jnp.where(small, both[:block], both[block:])


def local_part(query, key, value, decay, extra):
    tokens, width = query.shape
    pairs = width // LANES
    column = pl.BlockSpec((tokens, LANES), lambda p: (0, p))
    return pl.pallas_call(
        local_kernel,
        grid=(pairs,),
        in_specs=[column] * 4 + [pl.BlockSpec(extra.shape, lambda p: (0, 0))],
        out_specs=[
            column,
            pl.BlockSpec((tokens, 2 * LANES), lambda p: (0, p)),
            pl.BlockSpec((LANES, LANES), lambda p: (p, 0)),
            pl.BlockSpec((1, 1, LANES), lambda p: (p, 0, 0)),
        ],
        out_shape=[
            jax.ShapeDtypeStruct((tokens, width), jnp.float32),
            jax.ShapeDtypeStruct((tokens, 2 * width), jnp.bfloat16),
            jax.ShapeDtypeStruct((width, LANES), jnp.bfloat16),
            jax.ShapeDtypeStruct((pairs, 1, LANES), jnp.float32),
        ],
        name="local_part",
    )(query, key, value, decay, extra)


def exchange_kernel(
    n,
    state_ref,
    total_ref,
    out_ref,
    arrived,
    totals,
    ordered,
    before,
    outbound,
    send_state,
    recv_state,
    send_total,
    recv_total,
    send_back,
    recv_back,
):
    me = lax.axis_index("sp")
    rows = state_ref.shape[0] // n
    barrier = pltpu.get_barrier_semaphore()

    def greet(off, c):
        pl.semaphore_signal(
            barrier, inc=1, device_id={"sp": lax.rem(me + off, n)}, device_id_type=MESH
        )
        return c

    lax.fori_loop(1, n, greet, 0)
    pl.semaphore_wait(barrier, n - 1)

    def forth(off):
        to = lax.rem(me + off, n)
        first = pltpu.make_async_remote_copy(
            src_ref=state_ref.at[pl.ds(pl.multiple_of(to * rows, rows), rows)],
            dst_ref=arrived.at[off],
            send_sem=send_state.at[off],
            recv_sem=recv_state.at[off],
            device_id={"sp": to},
            device_id_type=MESH,
        )
        second = pltpu.make_async_remote_copy(
            src_ref=total_ref,
            dst_ref=totals.at[off],
            send_sem=send_total.at[off],
            recv_sem=recv_total.at[off],
            device_id={"sp": to},
            device_id_type=MESH,
        )
        return first, second

    def back(off):
        to = lax.rem(me + off, n)
        return pltpu.make_async_remote_copy(
            src_ref=outbound.at[to],
            dst_ref=out_ref.at[pl.ds(pl.multiple_of(me * rows, rows), rows)],
            send_sem=send_back.at[off],
            recv_sem=recv_back.at[off],
            device_id={"sp": to},
            device_id_type=MESH,
        )

    def start_forth(off, c):
        for copy in forth(off):
            copy.start()
        return c

    def wait_forth(off, c):
        for copy in forth(off):
            copy.wait()
        return c

    def start_back(off, c):
        back(off).start()
        return c

    def wait_back(off, c):
        back(off).wait()
        return c

    lax.fori_loop(1, n, start_forth, 0)
    mine = pl.ds(pl.multiple_of(me * rows, rows), rows)
    arrived[0] = state_ref[mine]
    totals[0] = total_ref[...]
    ordered[...] = jnp.zeros_like(ordered)
    lax.fori_loop(1, n, wait_forth, 0)
    group, shift = me * rows // LANES, lax.rem(me * rows, LANES)
    for k in range(n):
        ordered[k : k + 1] = totals[lax.rem(me - k + n, n), group]
    turned = pltpu.roll(ordered[...], lax.rem(LANES - shift, LANES), 1)
    weights = jnp.exp(turned.T)[:rows]
    half = lane_half(rows)
    carried = jnp.zeros((rows, LANES), jnp.float32)
    for k in range(n):
        before[k] = carried
        if k < n - 1:
            carried = weights[:, k : k + 1] * carried + arrived[lax.rem(me - k + n, n)].astype(
                jnp.float32
            )
    carried = jnp.zeros((rows, LANES), jnp.float32)
    for k in range(n - 1, -1, -1):
        outbound[k] = jnp.where(half, before[k], carried).astype(jnp.bfloat16)
        if k:
            carried = weights[:, k : k + 1] * carried + arrived[lax.rem(me - k + n, n)].astype(
                jnp.float32
            )
    lax.fori_loop(1, n, start_back, 0)
    out_ref[mine] = outbound[me]
    lax.fori_loop(1, n, wait_back, 0)


def exchange(state, total):
    n = lax.axis_size("sp")
    rows = state.shape[0] // n
    dma = pltpu.SemaphoreType.DMA((n,))
    return pl.pallas_call(
        functools.partial(exchange_kernel, n),
        in_specs=[pl.BlockSpec(memory_space=pltpu.VMEM)] * 2,
        out_specs=pl.BlockSpec(memory_space=pltpu.VMEM),
        out_shape=jax.ShapeDtypeStruct(state.shape, state.dtype),
        scratch_shapes=[
            pltpu.VMEM((n, rows, LANES), state.dtype),
            pltpu.VMEM((n,) + total.shape, jnp.float32),
            pltpu.VMEM((LANES, LANES), jnp.float32),
            pltpu.VMEM((n, rows, LANES), jnp.float32),
            pltpu.VMEM((n, rows, LANES), state.dtype),
            dma,
            dma,
            dma,
            dma,
            dma,
            dma,
        ],
        compiler_params=pltpu.CompilerParams(collective_id=0, has_side_effects=True),
        name="exchange",
    )(state, total)


def finish_kernel(local_ref, wide_ref, state_ref, logits_ref, gain_ref, out_ref):
    few = lane_half(KEY_HEAD_SIZE)
    first = state_ref[:KEY_HEAD_SIZE].astype(jnp.float32)
    second = state_ref[KEY_HEAD_SIZE:].astype(jnp.float32)
    states = jnp.concatenate(
        [
            jnp.where(few, first, 0.0),
            jnp.where(few, 0.0, pltpu.roll(second, KEY_HEAD_SIZE, 1)),
            jnp.where(few, pltpu.roll(first, KEY_HEAD_SIZE, 1), 0.0),
            jnp.where(few, 0.0, second),
        ],
        axis=0,
    ).astype(jnp.bfloat16)
    mixed = local_ref[...] + jnp.dot(wide_ref[...], states, preferred_element_type=jnp.float32)
    half = lane_half(mixed.shape[0])
    squares = mixed * mixed
    one = jnp.sum(jnp.where(half, squares, 0.0), axis=1, keepdims=True)
    two = jnp.sum(jnp.where(half, 0.0, squares), axis=1, keepdims=True)
    scale = jnp.where(
        half, lax.rsqrt(one / KEY_HEAD_SIZE + EPS), lax.rsqrt(two / KEY_HEAD_SIZE + EPS)
    )
    gate = jax.nn.silu(logits_ref[...].astype(jnp.float32))
    out_ref[...] = (mixed * scale * gain_ref[...] * gate).astype(jnp.bfloat16)


def finish_part(local, wide, state, logits, gain):
    tokens, width = local.shape
    column = pl.BlockSpec((tokens, LANES), lambda p: (0, p))
    return pl.pallas_call(
        finish_kernel,
        grid=(width // LANES,),
        in_specs=[
            column,
            pl.BlockSpec((tokens, 2 * LANES), lambda p: (0, p)),
            pl.BlockSpec((LANES, LANES), lambda p: (p, 0)),
            column,
            pl.BlockSpec((1, LANES), lambda p: (0, 0)),
        ],
        out_specs=column,
        out_shape=jax.ShapeDtypeStruct((tokens, width), jnp.bfloat16),
        name="finish_part",
    )(local, wide, state, logits, gain)


def expert_half(arrived, gate_half, up_half, down_half):
    flat_rows = arrived.reshape(-1, arrived.shape[-1])
    gate_part = jnp.dot(flat_rows, gate_half, preferred_element_type=jnp.float32)
    up_part = jnp.dot(flat_rows, up_half, preferred_element_type=jnp.float32)
    inner = (jax.nn.silu(gate_part) * up_part).astype(jnp.bfloat16)
    partial_out = jnp.dot(inner, down_half, preferred_element_type=jnp.float32).astype(jnp.bfloat16)
    return partial_out.reshape(arrived.shape)


def per_device(
    query_matrix,
    key_matrix,
    value_matrix,
    output_gate_logits,
    decay_preactivation,
    head_extra_decay,
    residual,
    head_norm_gain,
    output_projection_weight,
    mixer_norm_gain,
    routes,
    routing_weight,
    routed_gate_weight,
    routed_up_weight,
    routed_down_weight,
    common_gate_weight,
    common_up_weight,
    common_down_weight,
    final_norm_gain,
):
    local_out, wide, state, total = local_part(
        query_matrix, key_matrix, value_matrix, decay_preactivation, head_extra_decay
    )
    entered = exchange(state, total)
    gain = jnp.concatenate([head_norm_gain] * (LANES // KEY_HEAD_SIZE))[None]
    gated = finish_part(local_out, wide, entered, output_gate_logits, gain)
    projected = lax.psum_scatter(
        jnp.dot(gated, output_projection_weight, preferred_element_type=jnp.float32).astype(
            jnp.bfloat16
        ),
        "tp",
        scatter_dimension=0,
        tiled=True,
    ).astype(jnp.float32)
    normed = layer_norm(residual.astype(jnp.float32) + projected, mixer_norm_gain).astype(
        jnp.bfloat16
    )
    row_count = normed.shape[0]
    model_width = normed.shape[1]
    top_count = routes.shape[1]
    experts = lax.axis_size("sp")
    capacity = max(2, row_count * top_count // experts * 2)
    flat_expert = routes.reshape(-1)
    member = (flat_expert[:, None] == jnp.arange(experts, dtype=jnp.int32)[None, :]).astype(
        jnp.int32
    )
    rank_in = jnp.sum((jnp.cumsum(member, axis=0) - member) * member, axis=1)
    slot_of = flat_expert * capacity + rank_in
    source_row = (
        jnp.zeros((experts * capacity,), jnp.int32)
        .at[slot_of]
        .set(jnp.arange(row_count * top_count, dtype=jnp.int32) // top_count)
    )
    outbound = normed[source_row].reshape(experts, capacity, model_width)
    gate_half = routed_gate_weight[0]
    up_half = routed_up_weight[0]
    down_half = routed_down_weight[0]
    paired = lax.all_gather(
        lax.all_to_all(outbound, "sp", split_axis=0, concat_axis=0, tiled=True),
        "tp",
        axis=0,
        tiled=True,
    )
    partial_out = expert_half(paired, gate_half, up_half, down_half).astype(jnp.float32)
    summed = lax.psum_scatter(
        partial_out.astype(jnp.bfloat16), "tp", scatter_dimension=0, tiled=True
    )
    expert_out = lax.all_to_all(summed, "sp", split_axis=0, concat_axis=0, tiled=True)
    flat_out = expert_out.reshape(experts * capacity, model_width)
    picked = flat_out[slot_of].astype(jnp.float32).reshape(row_count, top_count, model_width)
    routed = jnp.einsum("rk,rkd->rd", routing_weight, picked)
    shared_gate_out = jnp.dot(normed, common_gate_weight, preferred_element_type=jnp.float32)
    shared_up_out = jnp.dot(normed, common_up_weight, preferred_element_type=jnp.float32)
    shared_inner = (jax.nn.silu(shared_gate_out) * shared_up_out).astype(jnp.bfloat16)
    feed = jnp.dot(shared_inner, common_down_weight, preferred_element_type=jnp.float32) + routed
    return layer_norm(normed.astype(jnp.float32) + feed, final_norm_gain).astype(jnp.bfloat16)


def solution(mesh):
    placed = (
        P("sp", "tp"),
        P("sp", "tp"),
        P("sp", "tp"),
        P("sp", "tp"),
        P("sp", "tp"),
        P("sp", "tp"),
        P(("sp", "tp"), None),
        P(),
        P("tp", None),
        P(),
        P(("sp", "tp"), None),
        P(("sp", "tp"), None),
        P("sp", None, "tp"),
        P("sp", None, "tp"),
        P("sp", "tp", None),
        P(),
        P(),
        P(),
        P(),
    )
    return jax.shard_map(
        per_device, mesh=mesh, in_specs=placed, out_specs=P(("sp", "tp"), None), check_vma=False
    )
```

time: 435 us -> 257 us (0.59)
  other arithmetic: 78.4 us -> 8.74 us
  waiting for transfers between devices: 135 us -> 72.9 us
  Pallas kernels: 0 us -> 47.4 us
  blocking collectives: 99.8 us -> 56.1 us
  matrix products: 57 us -> 31.4 us
  local copies, waits for them, and re-layouts: 36.9 us -> 15.1 us
    all_gather x2 -> x0, waiting for transfers between devices: 64.1 us -> none  [entering(): lax.all_gather(part.astype(kind), axis)]
    pallas_call x0 -> x3, Pallas kernels: none -> 47.4 us  [the longest x1 24.1 us: exchange(): pl.pallas_call(functools.partial(exchange_kernel, n), in_specs=[pl.BlockS...]
    all_gather x1 -> x0, blocking collectives: 43.6 us -> none  [entering(): lax.all_gather(part.astype(kind), axis)]
    select_n x32 -> x0, other arithmetic: 41.5 us -> none  [step(): return jax.tree.map(lambda a, b: jnp.where(reached, a, b), new, before)]
    dot_general x8 -> x0, matrix products: 24.8 us -> none  [the longest x1 5.11 us: block_products(): local_out = jnp.einsum('nhij,njhv->nihv', scores, value_f)]
    add x8 -> x0, other arithmetic: 10.7 us -> none  [carry_step(): return (jnp.exp(total)[..., None] * carried + summed, carried)]
    mul x6 -> x0, local copies, waits for them, and re-layouts: 7.2 us -> none  [the longest x1 2.85 us: block_products(): query_matrix.astype(jnp.float32).reshape(blocked_layout)]
    mul x2 -> x0, other arithmetic: 6.89 us -> none  [the longest x1 5.79 us: block_products(): query_head = query_float * jnp.exp(from_start)]
  transfers between devices with their start and end apart: 6 -> 4, of which waited for: 6 -> 4; matrix products, arithmetic and copies ran while one was open for 12% -> 2% of each run, Pallas kernels for 0% -> 0%
where the time goes in v1:
time: 257 us; the launch traced here: 252 us
  waiting for transfers between devices  72.9 us (28%)
  blocking collectives  56.1 us (22%)
  Pallas kernels  47.4 us (18%)
  matrix products  31.4 us (12%)
  local copies, waits for them, and re-layouts  15.1 us (6%)
  between operations  13.3 us (5%)
  other arithmetic  8.74 us (3%)
  starting transfers between devices  7.04 us (3%)
    all_to_all x1, blocking collectives, per_device(): lax.all_to_all(outbound, 'sp', split_axis=0, concat_axis=0, tiled=True)  56.1 us
    all_to_all x1, waiting for transfers between devices, per_device(): lax.all_to_all(summed, 'sp', split_axis=0, concat_axis=0, tiled=True)  41.1 us
    pallas_call x1, Pallas kernels, exchange(): pl.pallas_call(functools.partial(exchange_kernel, n), in_specs=[pl.BlockS...  24.1 us
    pallas_call x1, Pallas kernels, local_part(): pl.pallas_call(local_kernel, grid=(pairs,), in_specs=[column] * 4 + [pl.B...  16.4 us
    reduce_scatter x1, waiting for transfers between devices, per_device(): lax.psum_scatter(partial_out.astype(jnp.bfloat16), 'tp', scatter_dimensio...  13.4 us
    all_gather x1, waiting for transfers between devices, per_device(): lax.all_gather(lax.all_to_all(outbound, 'sp', split_axis=0, concat_axis=0...  12.1 us
    dot_general x1, matrix products, expert_half(): jnp.dot(inner, down_half, preferred_element_type=jnp.float32)  10.1 us
    all_to_all x1, starting transfers between devices, per_device(): lax.all_to_all(summed, 'sp', split_axis=0, concat_axis=0, tiled=True)  6.95 us
  transfers between devices with their start and end apart: 4, of which 4 were waited for; matrix products, arithmetic and copies ran while one was open for 2% of the time, Pallas kernels for 0%

profile of v1, /device:TPU:0, one launch (start us, length us, event | category | flops | bytes accessed | tf_op | source)
XLA Modules:
  0.0 252.0 jit_solution(14890889365379662625)
XLA Ops:
  6.5 1.6 copy.26.extra_ref
  9.5 16.4 %local_part.1 = (f32[256,1024]{1,0:T(8,128)}, bf16[256,2048]{1,0:T(8,128)(2,1)}, bf16[1024,128]{1,0:T(8,128)(2,1)}, f32[8,1,128]{2,1,0:T(1,128)}) custom-call(bf16[256,1024]{1,0:T(8,128)(2,1)} %q_ref.1, bf16[256,1024]{1,0:T(8,128)(2,1)} %k_ref.1, bf16[256,1024]{1,0:T(8,128)(2,1)} %v_ref.1, bf16[256,1024]{1,0:T(8,128)(2,1)} %decay_ref.1, ...), custom_call_target="tpu_custom_call" | custom-call | tf_op jit(solution)/shard_map/local_part/pallas_call | solution.py:116
  25.9 24.1 %exchange.1.state_ref = bf16[1024,128]{1,0:T(8,128)(2,1)} custom-call(bf16[1024,128]{1,0:T(8,128)(2,1)} %get-tuple-element.11.state_ref, f32[8,1,128]{2,1,0:T(1,128)} %get-tuple-element.12.total_ref), custom_call_target="tpu_custom_call" | custom-call | tf_op jit(solution)/shard_map/exchange/pallas_call | solution.py:250
  50.0 6.9 %finish_part.1 = bf16[256,1024]{1,0:T(8,128)(2,1)} custom-call(f32[256,1024]{1,0:T(8,128)} %get-tuple-element.9.local_ref, bf16[256,2048]{1,0:T(8,128)(2,1)} %get-tuple-element.10.wide_ref, bf16[1024,128]{1,0:T(8,128)(2,1)} %exchange.1.state_ref, bf16[256,1024]{1,0:T(8,128)(2,1)} %logits_ref.1, f32[1,128]{1,0:T(1,128)} %maximum_bitcast_fusion.gain_ref), custom_call_target="tpu_custom_call" | custom-call | tf_op jit(solution)/shard_map/finish_part/pallas_call | solution.py:301
  56.9 4.7 %convolution_convert_fusion.1 = bf16[256,2048]{1,0:T(8,128)(2,1)} fusion(bf16[256,1024]{1,0:T(8,128)(2,1)} %finish_part.1, bf16[1024,2048]{1,0:T(8,128)(2,1)} %param.27), kind=kOutput, calls=%fused_computation.4 | convolution fusion | flops 1074266112 | bytes 5767168 | tf_op jit(solution)/shard_map/dot_general | solution.py:354
  63.2 1.4 scatter_custom_fusion
  64.6 6.3 %reduce-scatter.3.cloned.1.call-done = bf16[128,2048]{1,0:T(8,128)(2,1)} async-done(((bf16[256,2048]{1,0:T(8,128)(2,1)}), bf16[128,2048]{1,0:T(8,128)(2,1)}) %reduce-scatter.3.cloned.1.call-update) | async-done | bytes 524304 | tf_op jit(solution)/shard_map/reduce_scatter | solution.py:353
  70.9 1.3 fusion.10
  72.3 1.3 multiply_reduce_fusion.1
  73.9 3.3 %gather_fusion = bf16[512,2048]{1,0:T(8,128)(2,1)} fusion(bf16[128,2048]{1,0:T(8,128)(2,1)S(1)} %multiply_convert_fusion.2, s32[1024]{0:T(1024)S(1)} %pad_clamp_fusion.1), kind=kCustom, calls=%fused_computation | custom fusion | bytes 4196352 | tf_op jit(solution)/shard_map/gather | solution.py:380
  77.2 56.1 %all_to_all.10 = bf16[16,32,2048]{2,1,0:T(8,128)(2,1)} all-to-all(bf16[16,32,2048]{2,1,0:T(8,128)(2,1)} %bitcast.54), channel_id=1, replica_groups=mesh['sp'=16,'tp'=2] {'sp'}, dimensions={0} | all-to-all | bytes 4194304 | tf_op jit(solution)/shard_map/all_to_all | solution.py:385
  133.5 12.1 %all-gather.2.cloned.1.call-done = bf16[32,32,2048]{2,1,0:T(8,128)(2,1)} async-done(((bf16[16,32,2048]{2,1,0:T(8,128)(2,1)}), bf16[32,32,2048]{2,1,0:T(8,128)(2,1)}) %all-gather.2.cloned.1.call-update) | async-done | bytes 4194320 | tf_op jit(solution)/shard_map/all_gather | solution.py:384
  145.6 6.6 %fusion.2 = f32[1024,512]{1,0:T(8,128)} fusion(bf16[1024,2048]{1,0:T(8,128)(2,1)} %bitcast.60, bf16[1,2048,512]{2,1,0:T(8,128)(2,1)} %param.32), kind=kOutput, calls=%fused_computation.8 | convolution fusion | flops 2147483648 | bytes 8388608 | tf_op jit(solution)/shard_map/dot_general | solution.py:320
  152.1 10.1 %convolution_convert_fusion = bf16[1024,2048]{1,0:T(8,128)(2,1)} fusion(bf16[1,512,2048]{2,1,0:T(8,128)(2,1)S(1)} %copy-done, f32[1024,512]{1,0:T(8,128)} %fusion.2, bf16[1024,2048]{1,0:T(8,128)(2,1)} %bitcast.61, bf16[1,2048,512]{2,1,0:T(8,128)(2,1)} %param.31), kind=kOutput, calls=%fused_computation.3 | convolution fusion | flops 4300210176 | bytes 14680064 | tf_op jit(solution)/shard_map/dot_general | solution.py:322
  162.3 13.4 %reduce-scatter.5.cloned.1.call-done = bf16[16,32,2048]{2,1,0:T(8,128)(2,1)} async-done(((bf16[32,32,2048]{2,1,0:T(8,128)(2,1)}), bf16[16,32,2048]{2,1,0:T(8,128)(2,1)}) %reduce-scatter.5.cloned.1.call-update) | async-done | bytes 2097168 | tf_op jit(solution)/shard_map/reduce_scatter | solution.py:391
  175.6 7.0 %all-to-all-start.1 = ((bf16[16,32,2048]{2,1,0:T(8,128)(2,1)}), bf16[16,32,2048]{2,1,0:T(8,128)(2,1)}, u32[]{:S(2)}, u32[]{:S(2)}) async-start(bf16[16,32,2048]{2,1,0:T(8,128)(2,1)} %reduce-scatter.5.cloned.1.call-done), calls=%async_computation.3 | async-start | bytes 4194304 | tf_op jit(solution)/shard_map/all_to_all | solution.py:394
  182.8 2.0 fusion.28
  184.8 41.1 %all-to-all-done.1 = bf16[16,32,2048]{2,1,0:T(8,128)(2,1)} async-done(((bf16[16,32,2048]{2,1,0:T(8,128)(2,1)}), bf16[16,32,2048]{2,1,0:T(8,128)(2,1)}, u32[]{:S(2)}, u32[]{:S(2)}) %all-to-all-start.1) | async-done | bytes 2097184 | tf_op jit(solution)/shard_map/all_to_all | solution.py:394
  225.9 5.2 %gather_fusion.1 = bf16[256,2048]{1,0:T(8,128)(2,1)} fusion(bf16[512,2048]{1,0:T(8,128)(2,1)} %bitcast.10, s32[1024]{0:T(1024)S(1)} %pad_clamp_fusion), kind=kCustom, calls=%fused_computation.1 | custom fusion | bytes 2098176 | tf_op jit(solution)/shard_map/gather | solution.py:396
  231.1 2.5 %reshape.92 = bf16[128,2,2048]{2,1,0:T(2,128)(2,1)} reshape(bf16[256,2048]{1,0:T(8,128)(2,1)} %gather_fusion.1) | data formatting | bytes 2097152 | tf_op jit(solution)/shard_map/reshape | solution.py:396
  233.7 3.5 %fusion.29 = f32[128,1,2048]{2,1,0:T(1,128)} fusion(bf16[128,2,2048]{2,1,0:T(2,128)(2,1)} %reshape.92, bf16[128,2,1]{1,2,0:T(2,128)(2,1)S(1)} %copy.31), kind=kOutput, calls=%fused_computation.57 | convolution fusion | flops 1048576 | bytes 2097664 | tf_op jit(solution)/shard_map/rk,rkd->rd/dot_general | solution.py:397
  237.2 4.6 %fusion.27 = (f32[128]{0:T(128)S(1)}, f32[128,2048]{1,0:T(8,128)}) fusion(f32[128,1,2048]{2,1,0:T(1,128)} %fusion.29, bf16[512,2048]{1,0:T(8,128)(2,1)} %param.36, bf16[128,2048]{1,0:T(8,128)(2,1)S(1)} %multiply_convert_fusion.2, bf16[2048,512]{1,0:T(8,128)(2,1)} %param.35, f32[128,512]{1,0:T(8,128)S(1)} %fusion.28), kind=kOutput, calls=%fused_computation.55 | convolution fusion | flops 538312576 | bytes 7078400 | tf_op jit(solution)/shard_map/dot_general | solution.py:401
  241.8 1.5 multiply_reduce_fusion
  243.2 2.2 multiply_convert_fusion.1
  (44 shorter events, 3.5 us)
Async XLA Ops:
  6.5 145.6 %copy-start = (bf16[1,512,2048]{2,1,0:T(8,128)(2,1)S(1)}, bf16[1,512,2048]{2,1,0:T(8,128)(2,1)}, u32[]{:S(2)}) copy-start(bf16[1,512,2048]{2,1,0:T(8,128)(2,1)} %param.33) | copy-start | bytes 6291460
  6.5 64.4 %reduce-scatter.3.cloned.1.call-start = ((), (), s32[]{:S(2)}) async-start(), calls=%async_computation.4 | async-start | bytes 1572864 | tf_op jit(solution)/shard_map/reduce_scatter | solution.py:353
  56.9 4.7 %copy-start.5 = (s32[128,2]{0,1:T(2,128)S(1)}, s32[128,2]{0,1:T(2,128)}, u32[]{:S(2)}) copy-start(s32[128,2]{0,1:T(2,128)} %param.29) | copy-start | bytes 3076
  56.9 14.0 %copy-start.1 = (bf16[128,2048]{1,0:T(8,128)(2,1)S(1)}, bf16[128,2048]{1,0:T(8,128)(2,1)}, u32[]{:S(2)}) copy-start(bf16[128,2048]{1,0:T(8,128)(2,1)} %param.25) | copy-start | bytes 1572868
  61.5 12.1 %copy-start.3 = (f32[2048]{0:T(1024)S(1)}, f32[2048]{0:T(1024)}, u32[]{:S(2)}) copy-start(f32[2048]{0:T(1024)} %param.28) | copy-start | bytes 24580
  61.5 84.0 %all-gather.2.cloned.1.call-start = ((), (), s32[]{:S(2)}) async-start(), calls=%async_computation.5 | async-start | bytes 6291456 | tf_op jit(solution)/shard_map/all_gather | solution.py:384
  70.9 2.7 %copy-start.2 = (bf16[128,2048]{1,0:T(8,128)(2,1)S(1)}, bf16[128,2048]{1,0:T(8,128)(2,1)}, u32[]{:S(2)}) copy-start(bf16[128,2048]{1,0:T(8,128)(2,1)} %reduce-scatter.3.cloned.1.call-done) | copy-start | bytes 1572868
  133.4 42.2 %reduce-scatter.5.cloned.1.call-start = ((), (), s32[]{:S(2)}) async-start(), calls=%async_computation.6 | async-start | bytes 6291456 | tf_op jit(solution)/shard_map/reduce_scatter | solution.py:391
  162.3 20.3 %copy-start.6 = (f32[128,2]{0,1:T(2,128)S(1)}, f32[128,2]{0,1:T(2,128)}, u32[]{:S(2)}) copy-start(f32[128,2]{0,1:T(2,128)} %param.30) | copy-start | bytes 3076
  175.6 50.3 %all-to-all-start.1 = ((bf16[16,32,2048]{2,1,0:T(8,128)(2,1)}), bf16[16,32,2048]{2,1,0:T(8,128)(2,1)}, u32[]{:S(2)}, u32[]{:S(2)}) async-start(bf16[16,32,2048]{2,1,0:T(8,128)(2,1)} %reduce-scatter.5.cloned.1.call-done), calls=%async_computation.3 | async-start | bytes 4194304 | tf_op jit(solution)/shard_map/all_to_all | solution.py:394
  237.2 6.1 %copy-start.4 = (f32[2048]{0:T(1024)S(1)}, f32[2048]{0:T(1024)}, u32[]{:S(2)}) copy-start(f32[2048]{0:T(1024)} %param.37) | copy-start | bytes 24580
Sparse Core Ops, SparseCore 0:
  61.7 9.1 reduce-scatter.2
  133.5 11.9 all-gather.1
  162.4 13.2 reduce-scatter.4

commit v2 on v1

--- a/solution.py
+++ b/solution.py
@@ -314,13 +314,185 @@
     )(local, wide, state, logits, gain)
 
 
-def expert_half(arrived, gate_half, up_half, down_half):
-    flat_rows = arrived.reshape(-1, arrived.shape[-1])
-    gate_part = jnp.dot(flat_rows, gate_half, preferred_element_type=jnp.float32)
-    up_part = jnp.dot(flat_rows, up_half, preferred_element_type=jnp.float32)
-    inner = (jax.nn.silu(gate_part) * up_part).astype(jnp.bfloat16)
-    partial_out = jnp.dot(inner, down_half, preferred_element_type=jnp.float32).astype(jnp.bfloat16)
-    return partial_out.reshape(arrived.shape)
+GROUP = 4
+
+
+def expert_kernel(
+    n,
+    sent_ref,
+    gate_hbm,
+    up_hbm,
+    down_hbm,
+    result_ref,
+    rows_in,
+    gate_ref,
+    up_ref,
+    down_ref,
+    kept,
+    given,
+    taken,
+    summed,
+    send_out,
+    recv_out,
+    send_row,
+    recv_row,
+    send_part,
+    recv_part,
+    send_back,
+    recv_back,
+    local,
+):
+    me, core = lax.axis_index("sp"), lax.axis_index("tp")
+    groups = n // GROUP
+    capacity, width = sent_ref.shape[1:]
+    peer = {"tp": 1 - core}
+
+    def target(off):
+        high = lax.rem(me // GROUP + off // GROUP, groups)
+        return high * GROUP + lax.rem(lax.rem(me, GROUP) + lax.rem(off, GROUP), GROUP)
+
+    def origin(off):
+        high = lax.rem(me // GROUP - off // GROUP + groups, groups)
+        return high * GROUP + lax.rem(lax.rem(me, GROUP) - lax.rem(off, GROUP) + GROUP, GROUP)
+
+    def remote(source, destination, send, recv, device):
+        return pltpu.make_async_remote_copy(
+            src_ref=source,
+            dst_ref=destination,
+            send_sem=send,
+            recv_sem=recv,
+            device_id=device,
+            device_id_type=MESH,
+        )
+
+    def outward(off):
+        return remote(
+            sent_ref.at[target(off)],
+            rows_in.at[off // GROUP, 0, lax.rem(off, GROUP)],
+            send_out.at[off],
+            recv_out.at[off],
+            {"sp": target(off)},
+        )
+
+    def homeward(off):
+        return remote(
+            summed.at[off // GROUP, lax.rem(off, GROUP)],
+            result_ref.at[me],
+            send_back.at[off],
+            recv_back.at[off],
+            {"sp": origin(off)},
+        )
+
+    loads = [
+        pltpu.make_async_copy(gate_hbm, gate_ref, local.at[0]),
+        pltpu.make_async_copy(up_hbm, up_ref, local.at[1]),
+        pltpu.make_async_copy(down_hbm, down_ref, local.at[2]),
+        pltpu.make_async_copy(sent_ref.at[me], rows_in.at[0, 0, 0], local.at[3]),
+    ]
+    for load in loads:
+        load.start()
+    barrier = pltpu.get_barrier_semaphore()
+
+    def greet(off, c):
+        pl.semaphore_signal(barrier, inc=1, device_id={"sp": target(off)}, device_id_type=MESH)
+        return c
+
+    lax.fori_loop(1, n, greet, 0)
+    pl.semaphore_signal(barrier, inc=1, device_id=peer, device_id_type=MESH)
+    pl.semaphore_wait(barrier, n)
+
+    def start_outward(off, c):
+        outward(off).start()
+        return c
+
+    lax.fori_loop(1, n, start_outward, 0)
+    for load in loads:
+        load.wait()
+
+    def arrive(off, c):
+        outward(off).wait_recv()
+        return c
+
+    def start_homeward(off, c):
+        homeward(off).start()
+        return c
+
+    def step(group, c):
+        begin = group * GROUP
+        skip = 1 - (group + groups - 1) // groups
+        lax.fori_loop(begin + skip, begin + GROUP, arrive, 0)
+        share = remote(
+            rows_in.at[group, 0],
+            rows_in.at[group, 1],
+            send_row.at[group],
+            recv_row.at[group],
+            peer,
+        )
+        share.start()
+        share.wait()
+        rows = rows_in[group].reshape(2 * GROUP * capacity, width)
+        gate = jnp.dot(rows, gate_ref[...], preferred_element_type=jnp.float32)
+        up = jnp.dot(rows, up_ref[...], preferred_element_type=jnp.float32)
+        inner = (jax.nn.silu(gate) * up).astype(jnp.bfloat16)
+        part = jnp.dot(inner, down_ref[...], preferred_element_type=jnp.float32)
+        part = part.astype(jnp.bfloat16).reshape(2, GROUP, capacity, width)
+        given[group] = part[1]
+        kept[...] = part[0]
+        trade = remote(
+            given.at[group], taken.at[group], send_part.at[group], recv_part.at[group], peer
+        )
+        trade.start()
+        trade.wait()
+        summed[group] = (
+            kept[...].astype(jnp.float32) + taken[group].astype(jnp.float32)
+        ).astype(jnp.bfloat16)
+        lax.fori_loop(begin + skip, begin + GROUP, start_homeward, 0)
+        return c
+
+    lax.fori_loop(0, groups, step, 0)
+    result_ref[me] = summed[0, 0]
+
+    def finish(off, c):
+        outward(off).wait_send()
+        homeward(off).wait()
+        return c
+
+    lax.fori_loop(1, n, finish, 0)
+
+
+def expert_exchange(sent, gate_half, up_half, down_half):
+    n, capacity, width = sent.shape
+    groups = n // GROUP
+    block = (groups, GROUP, capacity, width)
+    each, few = pltpu.SemaphoreType.DMA((n,)), pltpu.SemaphoreType.DMA((groups,))
+    vmem, anywhere = pl.BlockSpec(memory_space=pltpu.VMEM), pl.BlockSpec(memory_space=pl.ANY)
+    return pl.pallas_call(
+        functools.partial(expert_kernel, n),
+        in_specs=[vmem] + [anywhere] * 3,
+        out_specs=vmem,
+        out_shape=jax.ShapeDtypeStruct(sent.shape, sent.dtype),
+        scratch_shapes=[
+            pltpu.VMEM((groups, 2) + block[1:], sent.dtype),
+            pltpu.VMEM(gate_half.shape, gate_half.dtype),
+            pltpu.VMEM(up_half.shape, up_half.dtype),
+            pltpu.VMEM(down_half.shape, down_half.dtype),
+            pltpu.VMEM(block[1:], sent.dtype),
+            pltpu.VMEM(block, sent.dtype),
+            pltpu.VMEM(block, sent.dtype),
+            pltpu.VMEM(block, sent.dtype),
+            each,
+            each,
+            few,
+            few,
+            few,
+            few,
+            each,
+            each,
+            pltpu.SemaphoreType.DMA((4,)),
+        ],
+        compiler_params=pltpu.CompilerParams(collective_id=1, has_side_effects=True),
+        name="expert_exchange",
+    )(sent, gate_half, up_half, down_half)
 
 
 def per_device(
@@ -381,17 +553,7 @@
     gate_half = routed_gate_weight[0]
     up_half = routed_up_weight[0]
     down_half = routed_down_weight[0]
-    paired = lax.all_gather(
-        lax.all_to_all(outbound, "sp", split_axis=0, concat_axis=0, tiled=True),
-        "tp",
-        axis=0,
-        tiled=True,
-    )
-    partial_out = expert_half(paired, gate_half, up_half, down_half).astype(jnp.float32)
-    summed = lax.psum_scatter(
-        partial_out.astype(jnp.bfloat16), "tp", scatter_dimension=0, tiled=True
-    )
-    expert_out = lax.all_to_all(summed, "sp", split_axis=0, concat_axis=0, tiled=True)
+    expert_out = expert_exchange(outbound, gate_half, up_half, down_half)
     flat_out = expert_out.reshape(experts * capacity, model_width)
     picked = flat_out[slot_of].astype(jnp.float32).reshape(row_count, top_count, model_width)
     routed = jnp.einsum("rk,rkd->rd", routing_weight, picked)

time: 257 us -> 217 us (0.84); the launches traced: 252 us -> 217 us
  Pallas kernels: 47.4 us -> 160 us
  waiting for transfers between devices: 72.9 us -> 5.97 us
  blocking collectives: 56.1 us -> 0 us
  matrix products: 31.4 us -> 13 us
  starting transfers between devices: 7.04 us -> 0.01 us
    pallas_call x0 -> x1, Pallas kernels: none -> 113 us  [expert_exchange(): pl.pallas_call(functools.partial(expert_kernel, n), in_specs=[vmem] + [an...]
    all_to_all x1 -> x0, blocking collectives: 56.1 us -> none  [per_device(): lax.all_to_all(outbound, 'sp', split_axis=0, concat_axis=0, tiled=True)]
    all_to_all x1 -> x0, waiting for transfers between devices: 41.1 us -> none  [per_device(): lax.all_to_all(summed, 'sp', split_axis=0, concat_axis=0, tiled=True)]
    dot_general x2 -> x0, matrix products: 16.7 us -> none  [the longest x1 10.1 us: expert_half(): jnp.dot(inner, down_half, preferred_element_type=jnp.float32)]
    reduce_scatter x1 -> x0, waiting for transfers between devices: 13.4 us -> none  [per_device(): lax.psum_scatter(partial_out.astype(jnp.bfloat16), 'tp', scatter_dimensio...]
    all_gather x1 -> x0, waiting for transfers between devices: 12.1 us -> none  [per_device(): lax.all_gather(lax.all_to_all(outbound, 'sp', split_axis=0, concat_axis=0...]
    all_to_all x1 -> x0, starting transfers between devices: 6.95 us -> none  [per_device(): lax.all_to_all(summed, 'sp', split_axis=0, concat_axis=0, tiled=True)]
  transfers between devices with their start and end apart: 4 -> 1, of which waited for: 4 -> 1; matrix products, arithmetic and copies ran while one was open for 2% -> 2% of each run, Pallas kernels for 0% -> 0%
where the time goes in v2:
time: 217 us
  Pallas kernels  160 us (74%)
  local copies, waits for them, and re-layouts  15.3 us (7%)
  between operations  13.6 us (6%)
  matrix products  13 us (6%)
  other arithmetic  8.74 us (4%)
  waiting for transfers between devices  5.97 us (3%)
    pallas_call x1, Pallas kernels, expert_exchange(): pl.pallas_call(functools.partial(expert_kernel, n), in_specs=[vmem] + [an...  113 us
    pallas_call x1, Pallas kernels, exchange(): pl.pallas_call(functools.partial(exchange_kernel, n), in_specs=[pl.BlockS...  24.1 us
    pallas_call x1, Pallas kernels, local_part(): pl.pallas_call(local_kernel, grid=(pairs,), in_specs=[column] * 4 + [pl.B...  16.4 us
    pallas_call x1, Pallas kernels, finish_part(): pl.pallas_call(finish_kernel, grid=(width // LANES,), in_specs=[column, p...  6.89 us
    reduce_scatter x1, waiting for transfers between devices, per_device(): lax.psum_scatter(jnp.dot(gated, output_projection_weight, preferred_eleme...  5.96 us
    gather x1, local copies, waits for them, and re-layouts, per_device(): flat_out[slot_of].astype(jnp.float32)  5.21 us
    dot_general x1, matrix products, per_device(): jnp.dot(gated, output_projection_weight, preferred_element_type=jnp.float32)  4.65 us
  transfers between devices with their start and end apart: 1, of which 1 were waited for; matrix products, arithmetic and copies ran while one was open for 2% of the time, Pallas kernels for 0%

profile of v2, /device:TPU:0, one launch (start us, length us, event | category | flops | bytes accessed | tf_op | source)
XLA Modules:
  0.0 216.8 jit_solution(4023506712270147756)
XLA Ops:
  6.5 1.6 copy.21.extra_ref
  8.2 1.3 maximum_bitcast_fusion.gain_ref
  9.5 16.4 %local_part.1 = (f32[256,1024]{1,0:T(8,128)}, bf16[256,2048]{1,0:T(8,128)(2,1)}, bf16[1024,128]{1,0:T(8,128)(2,1)}, f32[8,1,128]{2,1,0:T(1,128)}) custom-call(bf16[256,1024]{1,0:T(8,128)(2,1)} %q_ref.1, bf16[256,1024]{1,0:T(8,128)(2,1)} %k_ref.1, bf16[256,1024]{1,0:T(8,128)(2,1)} %v_ref.1, bf16[256,1024]{1,0:T(8,128)(2,1)} %decay_ref.1, ...), custom_call_target="tpu_custom_call" | custom-call | tf_op jit(solution)/shard_map/local_part/pallas_call | solution.py:116
  25.9 24.1 %exchange.1.state_ref = bf16[1024,128]{1,0:T(8,128)(2,1)} custom-call(bf16[1024,128]{1,0:T(8,128)(2,1)} %get-tuple-element.11.state_ref, f32[8,1,128]{2,1,0:T(1,128)} %get-tuple-element.12.total_ref), custom_call_target="tpu_custom_call" | custom-call | tf_op jit(solution)/shard_map/exchange/pallas_call | solution.py:250
  50.0 6.9 %finish_part.1 = bf16[256,1024]{1,0:T(8,128)(2,1)} custom-call(f32[256,1024]{1,0:T(8,128)} %get-tuple-element.9.local_ref, bf16[256,2048]{1,0:T(8,128)(2,1)} %get-tuple-element.10.wide_ref, bf16[1024,128]{1,0:T(8,128)(2,1)} %exchange.1.state_ref, bf16[256,1024]{1,0:T(8,128)(2,1)} %logits_ref.1, f32[1,128]{1,0:T(1,128)} %maximum_bitcast_fusion.gain_ref), custom_call_target="tpu_custom_call" | custom-call | tf_op jit(solution)/shard_map/finish_part/pallas_call | solution.py:301
  56.9 4.6 %convolution_convert_fusion = bf16[256,2048]{1,0:T(8,128)(2,1)} fusion(bf16[256,1024]{1,0:T(8,128)(2,1)} %finish_part.1, bf16[1024,2048]{1,0:T(8,128)(2,1)} %param.27), kind=kOutput, calls=%fused_computation.3 | convolution fusion | flops 1074266112 | bytes 5767168 | tf_op jit(solution)/shard_map/dot_general | solution.py:526
  62.0 0.6 reduce-window.6
  62.6 0.2 slice_reduce_fusion
  62.9 0.1 mul.73
  63.1 0.2 copy.26
  63.3 1.6 scatter_custom_fusion
  65.0 6.0 %reduce-scatter.2.cloned.1.call-done = bf16[128,2048]{1,0:T(8,128)(2,1)} async-done(((bf16[256,2048]{1,0:T(8,128)(2,1)}), bf16[128,2048]{1,0:T(8,128)(2,1)}) %reduce-scatter.2.cloned.1.call-update) | async-done | bytes 524304 | tf_op jit(solution)/shard_map/reduce_scatter | solution.py:525
  70.9 1.3 fusion.3
  72.3 1.3 multiply_reduce_fusion.1
  73.6 0.3 multiply_convert_fusion.1
  73.9 3.3 %gather_fusion = bf16[512,2048]{1,0:T(8,128)(2,1)} fusion(bf16[128,2048]{1,0:T(8,128)(2,1)S(1)} %multiply_convert_fusion.1, s32[1024]{0:T(1024)S(1)} %pad_clamp_fusion.1), kind=kCustom, calls=%fused_computation | custom fusion | bytes 4196352 | tf_op jit(solution)/shard_map/gather | solution.py:552
  77.2 112.9 %expert_exchange.1 = bf16[16,32,2048]{2,1,0:T(8,128)(2,1)} custom-call(bf16[16,32,2048]{2,1,0:T(8,128)(2,1)} %bitcast.41, bf16[2048,512]{1,0:T(8,128)(2,1)} %bitcast.42, bf16[2048,512]{1,0:T(8,128)(2,1)} %bitcast.43, bf16[512,2048]{1,0:T(8,128)(2,1)} %bitcast.44), custom_call_target="tpu_custom_call" | custom-call | tf_op jit(solution)/shard_map/expert_exchange/pallas_call | solution.py:469
  190.1 5.2 %gather_fusion.1 = bf16[256,2048]{1,0:T(8,128)(2,1)} fusion(bf16[512,2048]{1,0:T(8,128)(2,1)} %bitcast.40, s32[1024]{0:T(1024)S(1)} %pad_clamp_fusion), kind=kCustom, calls=%fused_computation.1 | custom fusion | bytes 2098176 | tf_op jit(solution)/shard_map/gather | solution.py:558
  195.3 2.5 %reshape.84 = bf16[128,2,2048]{2,1,0:T(2,128)(2,1)} reshape(bf16[256,2048]{1,0:T(8,128)(2,1)} %gather_fusion.1) | data formatting | bytes 2097152 | tf_op jit(solution)/shard_map/reshape | solution.py:558
  197.9 2.1 fusion.18
  200.0 2.2 %fusion.19 = f32[128,1,2048]{2,1,0:T(1,128)} fusion(bf16[128,2,2048]{2,1,0:T(2,128)(2,1)S(1)} %copy-done.3, bf16[128,2,1]{1,2,0:T(2,128)(2,1)S(1)} %copy.26), kind=kOutput, calls=%fused_computation.49 | convolution fusion | flops 1048576 | bytes 2097664 | tf_op jit(solution)/shard_map/rk,rkd->rd/dot_general | solution.py:559
  202.2 4.0 %fusion.17 = (f32[128]{0:T(128)S(1)}, f32[128,2048]{1,0:T(8,128)}) fusion(f32[128,1,2048]{2,1,0:T(1,128)} %fusion.19, bf16[512,2048]{1,0:T(8,128)(2,1)S(1)} %copy-done, bf16[128,2048]{1,0:T(8,128)(2,1)S(1)} %multiply_convert_fusion.1, bf16[2048,512]{1,0:T(8,128)(2,1)} %param.35, f32[128,512]{1,0:T(8,128)S(1)} %fusion.18), kind=kOutput, calls=%fused_computation.47 | convolution fusion | flops 538312576 | bytes 7078400 | tf_op jit(solution)/shard_map/dot_general | solution.py:563
  206.2 1.5 multiply_reduce_fusion
  207.7 2.2 %multiply_convert_fusion = bf16[128,2048]{1,0:T(8,128)(2,1)} fusion(f32[128,2048]{1,0:T(8,128)} %get-tuple-element.14, f32[2048]{0:T(1024)S(1)} %copy-done.5, f32[128]{0:T(128)S(1)} %add_rsqrt_fusion, f32[128]{0:T(128)S(1)} %broadcast_multiply_fusion.1), kind=kLoop, calls=%fused_computation.8 | loop fusion | flops 1048576 | bytes 1582080 | tf_op jit(solution)/shard_map/convert_element_type | solution.py:564
  (36 shorter events, 0.8 us)
Async XLA Ops:
  6.5 195.7 %copy-start = (bf16[512,2048]{1,0:T(8,128)(2,1)S(1)}, bf16[512,2048]{1,0:T(8,128)(2,1)}, u32[]{:S(2)}) copy-start(bf16[512,2048]{1,0:T(8,128)(2,1)} %param.36) | copy-start | bytes 6291460
  6.5 64.4 %reduce-scatter.2.cloned.1.call-start = ((), (), s32[]{:S(2)}) async-start(), calls=%async_computation.1 | async-start | bytes 1572864 | tf_op jit(solution)/shard_map/reduce_scatter | solution.py:525
  56.9 4.7 %copy-start.6 = (s32[128,2]{0,1:T(2,128)S(1)}, s32[128,2]{0,1:T(2,128)}, u32[]{:S(2)}) copy-start(s32[128,2]{0,1:T(2,128)} %param.29) | copy-start | bytes 3076
  56.9 6.2 %copy-start.7 = (f32[128,2]{0,1:T(2,128)S(1)}, f32[128,2]{0,1:T(2,128)}, u32[]{:S(2)}) copy-start(f32[128,2]{0,1:T(2,128)} %param.30) | copy-start | bytes 3076
  56.9 14.1 %copy-start.1 = (bf16[128,2048]{1,0:T(8,128)(2,1)S(1)}, bf16[128,2048]{1,0:T(8,128)(2,1)}, u32[]{:S(2)}) copy-start(bf16[128,2048]{1,0:T(8,128)(2,1)} %param.25) | copy-start | bytes 1572868
  61.5 12.1 %copy-start.4 = (f32[2048]{0:T(1024)S(1)}, f32[2048]{0:T(1024)}, u32[]{:S(2)}) copy-start(f32[2048]{0:T(1024)} %param.28) | copy-start | bytes 24580
  70.9 2.7 %copy-start.2 = (bf16[128,2048]{1,0:T(8,128)(2,1)S(1)}, bf16[128,2048]{1,0:T(8,128)(2,1)}, u32[]{:S(2)}) copy-start(bf16[128,2048]{1,0:T(8,128)(2,1)} %reduce-scatter.2.cloned.1.call-done) | copy-start | bytes 1572868
  197.9 2.1 copy-start.3
  202.2 5.5 %copy-start.5 = (f32[2048]{0:T(1024)S(1)}, f32[2048]{0:T(1024)}, u32[]{:S(2)}) copy-start(f32[2048]{0:T(1024)} %param.37) | copy-start | bytes 24580
Sparse Core Ops, SparseCore 0:
  61.7 9.1 reduce-scatter.1
